TPU v7x, 256 devices: a whole 4x4x8 slice. The times are simulated.
256 devices in a mesh: ep: 64 (over z, x, core), tp: 4 (over y).
Axes of the slice: x: 4, y: 4, z: 8, core: 2. Of those that a mesh axis runs over, the one named last changes fastest.
Arguments:
- gate_branch: bfloat16 [32768, 2048], P(('ep', 'tp')), may hold values from -8 to 8
- rec_branch: bfloat16 [32768, 2048], P(('ep', 'tp')), may hold values from -6 to 6
- conv_weight: float32 [4, 2048], replicated, may hold values from -3 to 3
- gate_a: bfloat16 [8, 256, 256], replicated, may hold values from -0.375 to 0.375
- gate_x: bfloat16 [8, 256, 256], replicated, may hold values from -0.375 to 0.375
- decay_param: float32 [2048], replicated, as said below
- decay_shift: float32 [32768], P(('ep', 'tp')), may hold values from -0.6 to 0
- tokens: bfloat16 [32768, 2048], P(('ep', 'tp')), may hold values from -6 to 6
- routes: int32 [32768, 2], P(('ep', 'tp')), may hold values from 0 to 63, all different within a row; in each aligned block of 128 rows (0 to 127, 128 to 255, ...) at most 5 rows name the same one
- route_weight: float32 [32768, 2], P(('ep', 'tp')), may hold values from 0.1 to 0.9
- norm_gain: float32 [2048], replicated, may hold values from 0.1 to 1.9
- w_gate: bfloat16 [64, 2048, 3584], P('ep', None, 'tp'), may hold values from -0.125 to 0.125
- w_up: bfloat16 [64, 2048, 3584], P('ep', None, 'tp'), may hold values from -0.125 to 0.125
- w_down: bfloat16 [64, 3584, 2048], P('ep', 'tp'), may hold values from -0.09375 to 0.09375
Outputs:
- mixed_out: bfloat16 [32768, 2048], P(('ep', 'tp'))
- expert_out: bfloat16 [32768, 2048], P(('ep', 'tp'))
Inputs may be any that keep to these rules, and one draw needn't show every extreme that they name: `routes`: in each aligned block of 128 rows (the rows of one device) no expert is named more than 5 times, and some block names some expert exactly 5 times; the experts of one row differ. 8 softplus(-decay_param) lies between 0.2 / 32768 and 0.07.
All inputs are finite; a program needn't handle non-finite values.
Results may differ from a plain program's by a relative error of at most 0.012.
Values may be sent and summed in bfloat16 or wider, within the bound.
A program may use at most 128 MiB of HBM per device.

v0:
```python
import math
import jax
import jax.numpy as jnp
from jax import lax
from jax.sharding import Mesh
from jax.sharding import PartitionSpec as P

EP_TP = ("ep_0", "ep_1", "ep_2", "tp")
EP = ("ep_0", "ep_1", "ep_2")
EPSILON = 1e-05


def passed_along(block, axis, distance):
    devices = range(lax.axis_size(axis))
    route = [(i - distance, i) for i in devices if i - distance in devices]
    return lax.ppermute(block, axis, route)


def neutral_like(array, identity):
    return jax.tree.map(
        lambda part, zero: jnp.zeros_like(part) + jnp.asarray(zero, part.dtype), array, identity
    )


def gathered_once(array, axis):
    leaves = jax.tree.leaves(array)
    sequence = sorted(range(len(leaves)), key=lambda k: -leaves[k].size)
    width = (1, *leaves[sequence[0]].shape)[-1]
    lines = [
        jnp.pad(leaves[k].reshape(-1), (0, -leaves[k].size % width)).reshape(-1, width)
        for k in sequence
    ]
    both, at, found = (lax.all_gather(jnp.concatenate(lines), axis), 0, {})
    for k, line in zip(sequence, lines):
        piece = both[:, at : at + len(line)].reshape(len(both), -1)
        found[k] = piece[:, : leaves[k].size].reshape(-1, *leaves[k].shape)
        at += len(line)
    numbers = iter(range(len(leaves)))
    return jax.tree.map(lambda _: found[next(numbers)], array)


def carried_in(array, axes, combine, identity):
    before = start = neutral_like(array, identity)
    subtotal = array
    for axis in reversed(axes):
        length, here = (lax.axis_size(axis), lax.axis_index(axis))
        pieces = gathered_once(subtotal, axis)
        inside, subtotal = (start, start)
        for k in range(length):
            passed = k < here
            subtotal = combine(subtotal, jax.tree.map(lambda part: part[k], pieces))
            inside = jax.tree.map(lambda new, old: jnp.where(passed, new, old), subtotal, inside)
        before = combine(inside, before)
    return before


def pair_combine(earlier, later):
    return (earlier[0] * later[0], later[0] * earlier[1] + later[1])


def short_conv(previous, current, conv_weight):
    tap_count = conv_weight.shape[0]
    row_count = current.shape[0]
    padded = jnp.concatenate([previous, current], 0)
    summed = jnp.zeros(current.shape, jnp.float32)
    for tap_index in range(tap_count):
        summed = summed + conv_weight[tap_index] * padded[tap_index : tap_index + row_count].astype(
            jnp.float32
        )
    return summed.astype(jnp.bfloat16)


def mixer_gates(conv_rows, gate_a, gate_x, decay_rate, shift_rows):
    row_count, width_all = conv_rows.shape
    block_count, block_width = (gate_a.shape[0], gate_a.shape[1])
    split_rows = conv_rows.reshape(row_count, block_count, block_width)
    pre_a = jnp.einsum("rnc,ncd->rnd", split_rows, gate_a, preferred_element_type=jnp.float32)
    pre_x = jnp.einsum("rnc,ncd->rnd", split_rows, gate_x, preferred_element_type=jnp.float32)
    recur_gate = jax.nn.sigmoid(pre_a.reshape(row_count, width_all))
    input_gate = jax.nn.sigmoid(pre_x.reshape(row_count, width_all))
    log_a = -decay_rate[None, :] * recur_gate + shift_rows[:, None]
    drive = jnp.sqrt(-jnp.expm1(2.0 * log_a)) * input_gate * conv_rows.astype(jnp.float32)
    return (log_a, drive)


def blocked_recurrence(decay, drive):
    row_count, width_all = decay.shape
    group = math.gcd(row_count, 8)
    block_count = row_count // group
    decay_blocks = decay.reshape(block_count, group, width_all)
    drive_blocks = drive.reshape(block_count, group, width_all)
    factors = [decay_blocks[:, 0]]
    states = [drive_blocks[:, 0]]
    for inner in range(1, group):
        factors.append(factors[-1] * decay_blocks[:, inner])
        states.append(decay_blocks[:, inner] * states[-1] + drive_blocks[:, inner])
    factor_inner = jnp.stack(factors, 1)
    state_inner = jnp.stack(states, 1)

    def carry_step(carried, totals):
        return (pair_combine(carried, totals), carried)

    start = (jnp.ones((width_all,), jnp.float32), jnp.zeros((width_all,), jnp.float32))
    _, before = lax.scan(carry_step, start, (factors[-1], states[-1]))
    factor_all = factor_inner * before[0][:, None, :]
    state_all = state_inner + factor_inner * before[1][:, None, :]
    return (factor_all.reshape(row_count, width_all), state_all.reshape(row_count, width_all))


def layer_scale(rows_in, norm_gain):
    values = rows_in.astype(jnp.float32)
    center = jnp.mean(values, -1, keepdims=True)
    spread = jnp.mean(jnp.square(values - center), -1, keepdims=True)
    return ((values - center) * lax.rsqrt(spread + EPSILON) * norm_gain).astype(jnp.bfloat16)


def slot_numbers(routes, block_rows, expert_count):
    row_count, top_count = routes.shape
    onehot = (routes[:, :, None] == jnp.arange(expert_count, dtype=jnp.int32)).astype(jnp.int32)
    ranked = (
        jnp.cumsum(
            onehot.reshape(row_count // block_rows, block_rows * top_count, expert_count), axis=1
        )
        - 1
    )
    return jnp.sum(ranked.reshape(row_count, top_count, expert_count) * onehot, -1)


def expert_hidden(rows_in, gate_part, up_part):
    return (
        jax.nn.silu(jnp.dot(rows_in, gate_part, preferred_element_type=jnp.float32))
        * jnp.dot(rows_in, up_part, preferred_element_type=jnp.float32)
    ).astype(jnp.bfloat16)


def shards(
    gate_branch,
    rec_branch,
    conv_weight,
    gate_a,
    gate_x,
    decay_param,
    decay_shift,
    tokens,
    routes,
    route_weight,
    norm_gain,
    w_gate,
    w_up,
    w_down,
):
    tap_count = conv_weight.shape[0]
    row_count, width_all = rec_branch.shape
    previous = passed_along(rec_branch[row_count - (tap_count - 1) :], EP_TP, 1)
    conv_rows = short_conv(previous, rec_branch, conv_weight)
    decay_rate = 8.0 * jax.nn.softplus(-decay_param)
    log_a, drive = mixer_gates(conv_rows, gate_a, gate_x, decay_rate, decay_shift)
    factor, local_state = blocked_recurrence(jnp.exp(log_a), drive)
    identity = (jnp.ones((width_all,), jnp.float32), jnp.zeros((width_all,), jnp.float32))
    carried = carried_in((factor[-1], local_state[-1]), EP_TP, pair_combine, identity)
    states = local_state + factor * carried[1][None, :]
    mixed_out = (states * jax.nn.gelu(gate_branch.astype(jnp.float32), approximate=True)).astype(
        jnp.bfloat16
    )
    ep_count = lax.axis_size(EP)
    block_rows, top_count = routes.shape
    capacity = max(2, block_rows * top_count * 5 // (4 * ep_count))
    normed = layer_scale(tokens, norm_gain)
    slots = slot_numbers(routes, block_rows, ep_count)
    row_ids = jnp.broadcast_to(jnp.arange(block_rows, dtype=jnp.int32)[:, None], routes.shape)
    flat = routes * capacity + slots
    table = jnp.full((ep_count * capacity,), block_rows, jnp.int32)
    table = table.at[flat.reshape(-1)].set(row_ids.reshape(-1))
    outgoing = jnp.take(normed, table, axis=0, mode="fill", fill_value=0)
    outgoing = outgoing.reshape(ep_count, capacity, width_all)
    arrived = lax.all_to_all(outgoing, EP, split_axis=0, concat_axis=0, tiled=True)
    hidden = expert_hidden(
        lax.all_gather(arrived.reshape(-1, width_all), "tp", axis=0, tiled=True), w_gate[0], w_up[0]
    )
    route_out = lax.psum_scatter(
        jnp.dot(hidden, w_down[0], preferred_element_type=jnp.float32).astype(jnp.bfloat16),
        "tp",
        scatter_dimension=0,
        tiled=True,
    )
    returned = lax.all_to_all(
        route_out.reshape(ep_count, capacity, width_all),
        EP,
        split_axis=0,
        concat_axis=0,
        tiled=True,
    )
    returned = returned.reshape(ep_count * capacity, width_all)
    picked = jnp.take(returned, flat.reshape(-1), axis=0).astype(jnp.float32)
    picked = picked.reshape(block_rows, top_count, width_all)
    expert_out = jnp.sum(picked * route_weight[:, :, None], axis=1).astype(jnp.bfloat16)
    return (mixed_out, expert_out)


def solution(mesh):
    split = Mesh(mesh.devices.reshape(8, 4, 2, mesh.shape["tp"]), ("ep_0", "ep_1", "ep_2", "tp"))
    return jax.shard_map(
        shards,
        mesh=split,
        in_specs=(
            P(EP_TP, None),
            P(EP_TP, None),
            P(),
            P(),
            P(),
            P(),
            P(EP_TP),
            P(EP_TP, None),
            P(EP_TP, None),
            P(EP_TP, None),
            P(),
            P(EP, None, "tp"),
            P(EP, None, "tp"),
            P(EP, "tp", None),
        ),
        out_specs=(P(EP_TP, None), P(EP_TP, None)),
        check_vma=False,
    )
```

profile of v0, /device:TPU:2, one launch (start us, length us, event | category | flops | bytes accessed | tf_op | source)
XLA Modules:
  0.0 314.5 jit_solution(11399140220905587292)
XLA Ops:
  7.2 0.9 copy.64
  8.3 0.6 reduce-window.6
  9.8 0.7 compare_and_fusion.1
  10.9 1.4 scatter_custom_fusion
  12.4 1.2 convert_reduce_fusion
  13.6 1.3 fusion.14
  14.9 1.4 fusion.16
  16.3 3.0 gather_fusion
  19.3 2.4 gather.13
  22.1 63.1 %all_to_all.10 = bf16[64,5,2048]{2,1,0:T(8,128)(2,1)S(1)} all-to-all(bf16[64,5,2048]{2,1,0:T(8,128)(2,1)S(1)} %broadcast_select_fusion.2), channel_id=1, replica_groups=mesh['ep_0'=8,'ep_1'=4,'ep_2'=2,'tp'=4] {'ep_0','ep_1','ep_2'}, dimensions={0} | all-to-all | bytes 2621440 | tf_op jit(solution)/shard_map/all_to_all | solution.py:176
  85.2 1.4 reshape.838
  86.7 0.8 slice.280
  87.8 3.7 %collective-permute-start = (bf16[3,2048]{0,1:T(8,128)(2,1)S(1)}, bf16[3,2048]{0,1:T(8,128)(2,1)S(1)}, u32[]{:S(2)}, u32[]{:S(2)}) collective-permute-start(bf16[3,2048]{0,1:T(8,128)(2,1)S(1)} %copy.55), channel_id=1, source_target_pairs={{0,1},{1,2},{2,3},{3,4},{4,5},{5,6},{6,7},{7,8},{8,9},{9,10},{10,1... | collective-permute-start | bytes 36872 | tf_op jit(solution)/shard_map/ppermute | solution.py:16
  91.5 0.6 pad_clamp_fusion
  92.1 1.3 copy.56
  93.6 0.7 copy.69
  94.3 0.7 copy.71
  95.1 12.4 %collective-permute-done = bf16[3,2048]{0,1:T(8,128)(2,1)S(1)} collective-permute-done((bf16[3,2048]{0,1:T(8,128)(2,1)S(1)}, bf16[3,2048]{0,1:T(8,128)(2,1)S(1)}, u32[]{:S(2)}, u32[]{:S(2)}) %collective-permute-start) | collective-permute-done | bytes 12320 | tf_op jit(solution)/shard_map/ppermute | solution.py:16
  107.5 2.1 add_convert_fusion
  109.6 0.8 copy-done.2
  110.4 0.5 fusion.11
  111.2 0.6 copy.63
  111.8 2.9 fusion.7
  114.7 1.5 copy.61
  116.3 3.0 fusion.24
  119.2 1.6 copy.62
  121.2 2.2 slice_add_fusion
  123.4 2.8 stack.4
  126.2 0.7 slice_multiply_fusion
  127.0 2.6 stack.5
  129.5 18.4 %all-gather.10.cloned.1.call-done = bf16[1280,2048]{1,0:T(8,128)(2,1)} async-done(((bf16[320,2048]{1,0:T(8,128)(2,1)}), bf16[1280,2048]{1,0:T(8,128)(2,1)}) %all-gather.10.cloned.1.call-update) | async-done | bytes 5242896 | tf_op jit(solution)/shard_map/all_gather | solution.py:178
  148.0 9.9 %fusion.2 = f32[1280,896]{1,0:T(8,128)} fusion(bf16[1280,2048]{1,0:T(8,128)(2,1)} %all-gather.10.cloned.1.call-done, bf16[1,2048,896]{2,1,0:T(8,128)(2,1)} %param.27), kind=kOutput, calls=%fused_computation.12 | convolution fusion | flops 4697620480 | bytes 13500416 | tf_op jit(solution)/shard_map/dot_general | solution.py:131
  157.9 17.6 %convolution_convert_fusion = bf16[1280,2048]{1,0:T(8,128)(2,1)} fusion(bf16[1,896,2048]{2,1,0:T(8,128)(2,1)} %param.29, f32[1280,896]{1,0:T(8,128)} %fusion.2, bf16[1280,2048]{1,0:T(8,128)(2,1)} %all-gather.10.cloned.1.call-done, bf16[1,2048,896]{2,1,0:T(8,128)(2,1)} %param.28), kind=kOutput, calls=%fused_computation.8 | convolution fusion | flops 9404743680 | bytes 22413312 | tf_op jit(solution)/shard_map/dot_general | solution.py:181
  175.6 0.8 copy-done.5
  176.4 7.8 %while.17 = (s32[]{:T(128)}, f32[2048]{0:T(1024)S(1)}, f32[2048]{0:T(1024)S(1)}, f32[16,2048]{1,0:T(8,128)S(1)}, f32[16,2048]{1,0:T(8,128)S(1)}, /*index=5*/f32[...) while((s32[]{:T(128)}, f32[2048]{0:T(1024)S(1)}, f32[2048]{0:T(1024)S(1)}, ...), condition=%wide.region_1.2_spmd.clone, body=%wide.region_0.1_spmd.clone.sunk | while | flops 10243 | bytes 131187 | solution.py:104
  184.2 1.5 multiply_bitcast_fusion
  185.8 12.5 %all-gather.4 = f32[4,2,2048]{2,1,0:T(2,128)S(1)} all-gather(f32[1,2,2048]{2,1,0:T(2,128)S(1)} %maximum_bitcast_fusion), channel_id=2, replica_groups=mesh['ep_0'=8,'ep_1'=4,'ep_2'=2,'tp'=4] {'tp'}, dimensions={0}, use_global_device_ids=true | all-gather | bytes 81920 | tf_op jit(solution)/shard_map/all_gather | solution.py:33
  198.4 1.8 all-gather.5
  200.3 11.9 %all-gather.6 = f32[4,2,2048]{2,1,0:T(2,128)S(1)} all-gather(f32[1,2,2048]{2,1,0:T(2,128)S(1)} %maximum_bitcast_fusion.2), channel_id=4, replica_groups=mesh['ep_0'=8,'ep_1'=4,'ep_2'=2,'tp'=4] {'ep_1'}, dimensions={0}, use_global_device_ids=true | all-gather | bytes 81920 | tf_op jit(solution)/shard_map/all_gather | solution.py:33
  212.2 24.6 %all-gather.7 = f32[8,2,2048]{2,1,0:T(2,128)S(1)} all-gather(f32[1,2,2048]{2,1,0:T(2,128)S(1)} %maximum_bitcast_fusion.3), channel_id=5, replica_groups=mesh['ep_0'=8,'ep_1'=4,'ep_2'=2,'tp'=4] {'ep_0'}, dimensions={0}, use_global_device_ids=true | all-gather | bytes 147456 | tf_op jit(solution)/shard_map/all_gather | solution.py:33
  236.8 3.4 %reshape.839 = bf16[64,5,2048]{2,1,0:T(8,128)(2,1)} reshape(bf16[320,2048]{1,0:T(8,128)(2,1)} %reduce-scatter.2.cloned.1.call-done) | data formatting | bytes 2621440 | tf_op jit(solution)/shard_map/reshape | solution.py:187
  240.3 6.4 %all-to-all-start.1 = ((bf16[64,5,2048]{2,1,0:T(8,128)(2,1)}), bf16[64,5,2048]{2,1,0:T(8,128)(2,1)}, u32[]{:S(2)}, u32[]{:S(2)}) async-start(bf16[64,5,2048]{2,1,0:T(8,128)(2,1)} %reshape.839), calls=%async_computation.2 | async-start | bytes 4194304 | tf_op jit(solution)/shard_map/all_to_all | solution.py:186
  247.0 1.3 fusion.23
  248.2 49.6 %all-to-all-done.1 = bf16[64,5,2048]{2,1,0:T(8,128)(2,1)} async-done(((bf16[64,5,2048]{2,1,0:T(8,128)(2,1)}), bf16[64,5,2048]{2,1,0:T(8,128)(2,1)}, u32[]{:S(2)}, u32[]{:S(2)}) %all-to-all-start.1) | async-done | bytes 1310752 | tf_op jit(solution)/shard_map/all_to_all | solution.py:186
  297.8 2.6 reshape.840
  300.4 1.6 gather_fusion.1
  302.0 0.7 gather.15
  302.8 4.9 %multiply_reduce_fusion = bf16[128,2048]{1,0:T(8,128)(2,1)} fusion(bf16[128,2,2048]{2,1,0:T(2,128)(2,1)S(1)} %gather.15, pred[128,2]{1,0:T(8,128)(4,1)S(1)} %copy-done.7, f32[128,2]{1,0:T(8,128)S(1)} %copy-done.4), kind=kLoop, calls=%fused_computation.14 | loop fusion | flops 1835008 | bytes 1574144 | tf_op jit(solution)/shard_map/reduce_sum | solution.py:196
  (142 shorter events, 10.8 us)
Async XLA Ops:
  7.2 103.2 %copy-start = (bf16[8,256,256]{2,1,0:T(8,128)(2,1)S(1)}, bf16[8,256,256]{2,1,0:T(8,128)(2,1)}, u32[]{:S(2)}) copy-start(bf16[8,256,256]{2,1,0:T(8,128)(2,1)} %param.19) | copy-start | bytes 3145732
  7.2 140.8 %all-gather.10.cloned.1.call-start = ((), (), s32[]{:S(2)}) async-start(), calls=%async_computation.3 | async-start | bytes 6553600 | tf_op jit(solution)/shard_map/all_gather | solution.py:178
  85.2 6.3 %copy-start.9 = (f32[2048]{0:T(1024)S(1)}, f32[2048]{0:T(1024)}, u32[]{:S(2)}) copy-start(f32[2048]{0:T(1024)} %param.21) | copy-start | bytes 24580
  85.2 6.3 %copy-start.8 = (f32[4,2048]{1,0:T(4,128)S(1)}, f32[4,2048]{1,0:T(4,128)}, u32[]{:S(2)}) copy-start(f32[4,2048]{1,0:T(4,128)} %param.18) | copy-start | bytes 98308
  85.2 8.3 %copy-start.10 = (f32[128]{0:T(128)S(1)}, f32[128]{0:T(128)}, u32[]{:S(2)}) copy-start(f32[128]{0:T(128)} %param.22) | copy-start | bytes 1540
  85.2 9.1 %copy-start.11 = (f32[128,2]{0,1:T(2,128)S(1)}, f32[128,2]{0,1:T(2,128)}, u32[]{:S(2)}) copy-start(f32[128,2]{0,1:T(2,128)} %param.25) | copy-start | bytes 3076
  86.6 150.2 %reduce-scatter.2.cloned.1.call-start = ((), (), s32[]{:S(2)}) async-start(), calls=%async_computation.4 | async-start | bytes 6553600 | tf_op jit(solution)/shard_map/reduce_scatter | solution.py:180
  87.8 19.7 %collective-permute-start = (bf16[3,2048]{0,1:T(8,128)(2,1)S(1)}, bf16[3,2048]{0,1:T(8,128)(2,1)S(1)}, u32[]{:S(2)}, u32[]{:S(2)}) collective-permute-start(bf16[3,2048]{0,1:T(8,128)(2,1)S(1)} %copy.55), channel_id=1, source_target_pairs={{0,1},{1,2},{2,3},{3,4},{4,5},{5,6},{6,7},{7,8},{8,9},{9,10},{10,1... | collective-permute-start | bytes 36872 | tf_op jit(solution)/shard_map/ppermute | solution.py:16
  109.6 0.8 copy-start.2
  175.5 0.9 copy-start.5
  175.5 1.0 copy-start.6
  236.8 10.2 %copy-start.3 = (bf16[128,2048]{1,0:T(8,128)(2,1)S(1)}, bf16[128,2048]{1,0:T(8,128)(2,1)}, u32[]{:S(2)}) copy-start(bf16[128,2048]{1,0:T(8,128)(2,1)} %param.16) | copy-start | bytes 1572868
  240.3 57.5 %all-to-all-start.1 = ((bf16[64,5,2048]{2,1,0:T(8,128)(2,1)}), bf16[64,5,2048]{2,1,0:T(8,128)(2,1)}, u32[]{:S(2)}, u32[]{:S(2)}) async-start(bf16[64,5,2048]{2,1,0:T(8,128)(2,1)} %reshape.839), calls=%async_computation.2 | async-start | bytes 4194304 | tf_op jit(solution)/shard_map/all_to_all | solution.py:186
  300.3 2.4 copy-start.4
  300.3 2.4 copy-start.7
  300.4 7.3 %copy-start.1 = (bf16[8,256,256]{2,1,0:T(8,128)(2,1)S(1)}, bf16[8,256,256]{2,1,0:T(8,128)(2,1)}, u32[]{:S(2)}) copy-start(bf16[8,256,256]{2,1,0:T(8,128)(2,1)} %param.19) | copy-start | bytes 3145732
Sparse Core Ops, SparseCore 0:
  86.8 61.1 all-gather.9
  175.6 53.6 reduce-scatter.1
where the time goes:
time: 316 us; the launch traced here: 315 us
  blocking collectives  114 us (36%)
  waiting for transfers between devices  80.4 us (25%)
  local copies, waits for them, and re-layouts  41.1 us (13%)
  matrix products  30.9 us (10%)
  other arithmetic  22.8 us (7%)
  between operations  14.6 us (5%)
  starting transfers between devices  10.1 us (3%)
    all_to_all x1, blocking collectives, shards(): lax.all_to_all(outgoing, EP, split_axis=0, concat_axis=0, tiled=True)  63.1 us
    all_gather x4, blocking collectives, gathered_once(): both, at, found = (lax.all_gather(jnp.concatenate(lines), axis), 0, {})  50.8 us
    all_to_all x1, waiting for transfers between devices, shards(): lax.all_to_all(route_out.reshape(ep_count, capacity, width_all), EP, spli...  49.6 us
    all_gather x1, waiting for transfers between devices, shards(): lax.all_gather(arrived.reshape(-1, width_all), 'tp', axis=0, tiled=True)  18.4 us
    dot_general x1, matrix products, shards(): jnp.dot(hidden, w_down[0], preferred_element_type=jnp.float32)  17.6 us
    ppermute x1, waiting for transfers between devices, passed_along(): return lax.ppermute(block, axis, route)  12.4 us
    dot_general x1, matrix products, expert_hidden(): jnp.dot(rows_in, gate_part, preferred_element_type=jnp.float32)  9.94 us
    dynamic_update_slice x32, local copies, waits for them, and re-layouts, blocked_recurrence(): _, before = lax.scan(carry_step, start, (factors[-1], states[-1]))  6.55 us
  transfers between devices with their start and end apart: 4, of which 3 were waited for; matrix products, arithmetic and copies ran while one was open for 11% of the time, Pallas kernels for 0%

commit v1 on v0

--- a/solution.py
+++ b/solution.py
@@ -8,6 +8,24 @@
 EP_TP = ("ep_0", "ep_1", "ep_2", "tp")
 EP = ("ep_0", "ep_1", "ep_2")
 EPSILON = 1e-05
+
+
+def gather_around(array, axis, dim):
+    ways, here, step = (lax.axis_size(axis), lax.axis_index(axis), array.shape[dim])
+    dims = [n * ways if d == dim else n for d, n in enumerate(array.shape)]
+    full = lax.dynamic_update_slice_in_dim(
+        jnp.zeros(dims, array.dtype), array, here * step, axis=dim
+    )
+    going_up = going_down = array
+    for far in range(1, ways // 2 + 1):
+        going_up = lax.ppermute(going_up, axis, [(d, (d + 1) % ways) for d in range(ways)])
+        full = lax.dynamic_update_slice_in_dim(full, going_up, (here - far) % ways * step, axis=dim)
+        if 2 * far < ways:
+            going_down = lax.ppermute(going_down, axis, [(d, (d - 1) % ways) for d in range(ways)])
+            full = lax.dynamic_update_slice_in_dim(
+                full, going_down, (here + far) % ways * step, axis=dim
+            )
+    return full
 
 
 def passed_along(block, axis, distance):
@@ -175,7 +193,7 @@
     outgoing = outgoing.reshape(ep_count, capacity, width_all)
     arrived = lax.all_to_all(outgoing, EP, split_axis=0, concat_axis=0, tiled=True)
     hidden = expert_hidden(
-        lax.all_gather(arrived.reshape(-1, width_all), "tp", axis=0, tiled=True), w_gate[0], w_up[0]
+        gather_around(arrived.reshape(-1, width_all), "tp", 0), w_gate[0], w_up[0]
     )
     route_out = lax.psum_scatter(
         jnp.dot(hidden, w_down[0], preferred_element_type=jnp.float32).astype(jnp.bfloat16),

time: 316 us -> 324 us (1.025)
  blocking collectives: 114 us -> 53.9 us
  waiting for transfers between devices: 80.4 us -> 110 us
  starting transfers between devices: 10.1 us -> 29.3 us
  local copies, waits for them, and re-layouts: 41.1 us -> 56.3 us
  other arithmetic: 22.8 us -> 28.8 us
    all_to_all x1 -> x0, blocking collectives: 63.1 us -> none  [shards(): lax.all_to_all(outgoing, EP, split_axis=0, concat_axis=0, tiled=True)]
    ppermute x0 -> x3, waiting for transfers between devices: none -> 30.1 us  [the longest x2 30.1 us: gather_around(): lax.ppermute(going_up, axis, [(d, (d + 1) % ways) for d in range(ways)])]
    all_to_all x0 -> x1, waiting for transfers between devices: none -> 19 us  [shards(): lax.all_to_all(outgoing, EP, split_axis=0, concat_axis=0, tiled=True)]
    all_gather x1 -> x0, waiting for transfers between devices: 18.4 us -> none  [shards(): lax.all_gather(arrived.reshape(-1, width_all), 'tp', axis=0, tiled=True)]
    all_to_all x0 -> x1, starting transfers between devices: none -> 12.1 us  [shards(): lax.all_to_all(outgoing, EP, split_axis=0, concat_axis=0, tiled=True)]
    dynamic_update_slice x0 -> x4, local copies, waits for them, and re-layouts: none -> 4.71 us  [the longest x2 3.08 us: gather_around(): lax.dynamic_update_slice_in_dim(full, going_up, (here - far) % ways * ste...]
    div x4, local copies, waits for them, and re-layouts: 2.65 us -> 7.05 us  [mixer_gates(): recur_gate = jax.nn.sigmoid(pre_a.reshape(row_count, width_all))]
    ppermute x0 -> x3, starting transfers between devices: none -> 3.88 us  [the longest x1 2 us: gather_around(): lax.ppermute(going_down, axis, [(d, (d - 1) % ways) for d in range(ways)])]
  transfers between devices with their start and end apart: 4 -> 7, of which waited for: 3 -> 5; matrix products, arithmetic and copies ran while one was open for 11% -> 16% of each run, Pallas kernels for 0% -> 0%
where the time goes in v1:
time: 324 us; the launch traced here: 323 us
  waiting for transfers between devices  110 us (34%)
  local copies, waits for them, and re-layouts  56.3 us (17%)
  blocking collectives  53.9 us (17%)
  starting transfers between devices  29.3 us (9%)
  matrix products  29 us (9%)
  other arithmetic  28.8 us (9%)
  between operations  14.6 us (5%)
    all_gather x4, blocking collectives, gathered_once(): both, at, found = (lax.all_gather(jnp.concatenate(lines), axis), 0, {})  53.9 us
    all_to_all x1, waiting for transfers between devices, shards(): lax.all_to_all(route_out.reshape(ep_count, capacity, width_all), EP, spli...  49.6 us
    ppermute x2, waiting for transfers between devices, gather_around(): lax.ppermute(going_up, axis, [(d, (d + 1) % ways) for d in range(ways)])  30.1 us
    all_to_all x1, waiting for transfers between devices, shards(): lax.all_to_all(outgoing, EP, split_axis=0, concat_axis=0, tiled=True)  19 us
    dot_general x1, matrix products, shards(): jnp.dot(hidden, w_down[0], preferred_element_type=jnp.float32)  17.5 us
    all_to_all x1, starting transfers between devices, shards(): lax.all_to_all(outgoing, EP, split_axis=0, concat_axis=0, tiled=True)  12.1 us
    ppermute x1, waiting for transfers between devices, passed_along(): return lax.ppermute(block, axis, route)  11.4 us
    all_to_all x1, starting transfers between devices, shards(): lax.all_to_all(route_out.reshape(ep_count, capacity, width_all), EP, spli...  9.76 us
  transfers between devices with their start and end apart: 7, of which 5 were waited for; matrix products, arithmetic and copies ran while one was open for 16% of the time, Pallas kernels for 0%

profile of v1, /device:TPU:2, one launch (start us, length us, event | category | flops | bytes accessed | tf_op | source)
XLA Modules:
  0.0 322.7 jit_solution(4474217241358795864)
XLA Ops:
  10.9 1.4 scatter_custom_fusion
  13.5 1.3 fusion.17
  14.9 1.4 fusion.19
  16.3 3.0 gather_fusion
  19.3 2.4 gather.13
  21.9 1.6 broadcast_select_fusion.2
  23.5 12.1 %all-to-all-start = ((bf16[64,5,2048]{2,1,0:T(8,128)(2,1)}), bf16[64,5,2048]{2,1,0:T(8,128)(2,1)S(1)}, u32[]{:S(2)}, u32[]{:S(2)}) async-start(bf16[64,5,2048]{2,1,0:T(8,128)(2,1)} %broadcast_select_fusion.2), calls=%async_computation | async-start | bytes 4194304 | tf_op jit(solution)/shard_map/all_to_all | solution.py:194
  37.5 3.5 %collective-permute-start = (bf16[3,2048]{0,1:T(8,128)(2,1)}, bf16[3,2048]{0,1:T(8,128)(2,1)}, u32[]{:S(2)}, u32[]{:S(2)}) collective-permute-start(bf16[3,2048]{0,1:T(8,128)(2,1)} %copy.55), channel_id=1, source_target_pairs={{0,1},{1,2},{2,3},{3,4},{4,5},{5,6},{6,7},{7,8},{8,9},{9,10},{10,1... | collective-permute-start | bytes 36872 | tf_op jit(solution)/shard_map/ppermute | solution.py:34
  41.6 2.0 copy.56
  45.2 11.4 %collective-permute-done = bf16[3,2048]{0,1:T(8,128)(2,1)} collective-permute-done((bf16[3,2048]{0,1:T(8,128)(2,1)}, bf16[3,2048]{0,1:T(8,128)(2,1)}, u32[]{:S(2)}, u32[]{:S(2)}) %collective-permute-start) | collective-permute-done | bytes 12320 | tf_op jit(solution)/shard_map/ppermute | solution.py:34
  56.6 4.6 %add_convert_fusion = bf16[128,2048]{0,1:T(8,128)(2,1)S(1)} fusion(bf16[128,2048]{0,1:T(8,128)(2,1)} %copy.56, bf16[3,2048]{0,1:T(8,128)(2,1)} %collective-permute-done, f32[2048]{0:T(1024)S(1)} %bitcast.221, f32[2048]{0:T(1024)S(1)} %bitcast.222, f32[2048]{0:T(1024)S(1)} %bitcast.220, f32[2048]{0:T(1024)S(1)} %bitcast.219), kind=kLoop, calls=%fused_computation.61 | loop fusion | flops 5505024 | bytes 1093632 | tf_op jit(solution)/shard_map/convert_element_type | solution.py:88
  62.0 1.5 fusion.14
  63.4 2.5 copy.59
  66.0 1.8 copy.63
  67.8 19.0 %all-to-all-done = bf16[64,5,2048]{2,1,0:T(8,128)(2,1)S(1)} async-done(((bf16[64,5,2048]{2,1,0:T(8,128)(2,1)}), bf16[64,5,2048]{2,1,0:T(8,128)(2,1)S(1)}, u32[]{:S(2)}, u32[]{:S(2)}) %all-to-all-start) | async-done | bytes 1310752 | tf_op jit(solution)/shard_map/all_to_all | solution.py:194
  86.8 1.4 reshape.838
  88.2 1.6 collective-permute-start.1
  89.8 2.8 fusion.10
  92.7 1.5 copy.61
  94.2 3.0 fusion.27
  97.2 1.7 copy.62
  100.0 1.4 add_exponential_fusion
  101.4 2.0 collective-permute-start.2
  103.4 15.4 %collective-permute-done.1 = bf16[320,2048]{1,0:T(8,128)(2,1)} collective-permute-done((bf16[320,2048]{1,0:T(8,128)(2,1)}, bf16[320,2048]{1,0:T(8,128)(2,1)}, u32[]{:S(2)}, u32[]{:S(2)}) %collective-permute-start.1) | collective-permute-done | bytes 1310752 | tf_op jit(solution)/shard_map/ppermute | solution.py:21
  119.1 2.3 slice_add_fusion
  121.4 2.9 stack.4
  124.3 1.7 slice_multiply_fusion
  126.0 3.9 %stack.5 = f32[16,8,2048]{2,1,0:T(8,128)} concatenate(f32[16,1,2048]{2,1,0:T(1,128)} %get-tuple-element.108, f32[16,1,2048]{2,1,0:T(1,128)} %get-tuple-element.94, f32[16,1,2048]{2,1,0:T(1,128)} %get-tuple-element.93, f32[16,1,2048]{2,1,0:T(1,128)} %get-tuple-element.92, f32[16,1,2048]{2,1,0:T(1,128)} %get-tuple-element.91, f32[16,1,2048]{2,1,0:T(1,128)} %get-tuple-element.90, ...), dimensions={1} | concatenate | bytes 2097152 | tf_op jit(solution)/shard_map/stack | solution.py:115
  130.8 1.6 constant_dynamic-update-slice_fusion.2
  132.4 1.5 constant_dynamic-update-slice_fusion.1
  133.9 14.7 %collective-permute-done.3 = bf16[320,2048]{1,0:T(8,128)(2,1)} collective-permute-done((bf16[320,2048]{1,0:T(8,128)(2,1)}, bf16[320,2048]{1,0:T(8,128)(2,1)}, u32[]{:S(2)}, u32[]{:S(2)}) %collective-permute-start.3) | collective-permute-done | bytes 1310752 | tf_op jit(solution)/shard_map/ppermute | solution.py:21
  148.6 1.5 constant_dynamic-update-slice_fusion
  150.0 2.4 copy-done.2
  152.4 7.1 %fusion.5 = f32[1280,896]{1,0:T(8,128)} fusion(bf16[1280,2048]{1,0:T(8,128)(2,1)S(1)} %constant_dynamic-update-slice_fusion, bf16[1,2048,896]{2,1,0:T(8,128)(2,1)S(1)} %copy-done.16), kind=kOutput, calls=%fused_computation.13 | convolution fusion | flops 4697620480 | bytes 13500416 | tf_op jit(solution)/shard_map/dot_general | solution.py:149
  159.5 17.5 %convolution_convert_fusion = bf16[1280,2048]{1,0:T(8,128)(2,1)} fusion(bf16[1,896,2048]{2,1,0:T(8,128)(2,1)} %param.29, f32[1280,896]{1,0:T(8,128)} %fusion.5, bf16[1280,2048]{1,0:T(8,128)(2,1)} %copy-done.2, bf16[1,2048,896]{2,1,0:T(8,128)(2,1)} %param.28), kind=kOutput, calls=%fused_computation.8 | convolution fusion | flops 9404743680 | bytes 22413312 | tf_op jit(solution)/shard_map/dot_general | solution.py:199
  178.1 7.8 %while.17 = (s32[]{:T(128)}, f32[2048]{0:T(1024)S(1)}, f32[2048]{0:T(1024)S(1)}, f32[16,2048]{1,0:T(8,128)S(1)}, f32[16,2048]{1,0:T(8,128)S(1)}, /*index=5*/f32[...) while((s32[]{:T(128)}, f32[2048]{0:T(1024)S(1)}, f32[2048]{0:T(1024)S(1)}, ...), condition=%wide.region_1.2_spmd.clone, body=%wide.region_0.1_spmd.clone.sunk | while | flops 10243 | bytes 131187 | solution.py:122
  185.9 1.5 multiply_bitcast_fusion
  187.4 12.4 %all-gather.4 = f32[4,2,2048]{2,1,0:T(2,128)S(1)} all-gather(f32[1,2,2048]{2,1,0:T(2,128)S(1)} %maximum_bitcast_fusion), channel_id=2, replica_groups=mesh['ep_0'=8,'ep_1'=4,'ep_2'=2,'tp'=4] {'tp'}, dimensions={0}, use_global_device_ids=true | all-gather | bytes 81920 | tf_op jit(solution)/shard_map/all_gather | solution.py:51
  199.9 1.8 all-gather.5
  201.8 13.4 %all-gather.6 = f32[4,2,2048]{2,1,0:T(2,128)S(1)} all-gather(f32[1,2,2048]{2,1,0:T(2,128)S(1)} %maximum_bitcast_fusion.2), channel_id=4, replica_groups=mesh['ep_0'=8,'ep_1'=4,'ep_2'=2,'tp'=4] {'ep_1'}, dimensions={0}, use_global_device_ids=true | all-gather | bytes 81920 | tf_op jit(solution)/shard_map/all_gather | solution.py:51
  215.3 26.3 %all-gather.7 = f32[8,2,2048]{2,1,0:T(2,128)S(1)} all-gather(f32[1,2,2048]{2,1,0:T(2,128)S(1)} %maximum_bitcast_fusion.3), channel_id=5, replica_groups=mesh['ep_0'=8,'ep_1'=4,'ep_2'=2,'tp'=4] {'ep_0'}, dimensions={0}, use_global_device_ids=true | all-gather | bytes 147456 | tf_op jit(solution)/shard_map/all_gather | solution.py:51
  241.6 3.5 %reshape.839 = bf16[64,5,2048]{2,1,0:T(8,128)(2,1)} reshape(bf16[320,2048]{1,0:T(8,128)(2,1)} %reduce-scatter.2.cloned.1.call-done) | data formatting | bytes 2621440 | tf_op jit(solution)/shard_map/reshape | solution.py:205
  245.1 9.8 %all-to-all-start.1 = ((bf16[64,5,2048]{2,1,0:T(8,128)(2,1)}), bf16[64,5,2048]{2,1,0:T(8,128)(2,1)}, u32[]{:S(2)}, u32[]{:S(2)}) async-start(bf16[64,5,2048]{2,1,0:T(8,128)(2,1)} %reshape.839), calls=%async_computation.2 | async-start | bytes 4194304 | tf_op jit(solution)/shard_map/all_to_all | solution.py:204
  255.2 1.3 fusion.26
  256.4 49.6 %all-to-all-done.1 = bf16[64,5,2048]{2,1,0:T(8,128)(2,1)} async-done(((bf16[64,5,2048]{2,1,0:T(8,128)(2,1)}), bf16[64,5,2048]{2,1,0:T(8,128)(2,1)}, u32[]{:S(2)}, u32[]{:S(2)}) %all-to-all-start.1) | async-done | bytes 1310752 | tf_op jit(solution)/shard_map/all_to_all | solution.py:204
  306.0 2.6 reshape.840
  308.6 1.6 gather_fusion.1
  311.0 4.9 %multiply_reduce_fusion = bf16[128,2048]{1,0:T(8,128)(2,1)} fusion(bf16[128,2,2048]{2,1,0:T(2,128)(2,1)S(1)} %gather.15, pred[128,2]{1,0:T(8,128)(4,1)S(1)} %copy-done.11, f32[128,2]{1,0:T(8,128)S(1)} %copy-done.8), kind=kLoop, calls=%fused_computation.15 | loop fusion | flops 1835008 | bytes 1574144 | tf_op jit(solution)/shard_map/reduce_sum | solution.py:214
  (161 shorter events, 21.4 us)
Async XLA Ops:
  7.2 54.8 %copy-start = (bf16[8,256,256]{2,1,0:T(8,128)(2,1)S(1)}, bf16[8,256,256]{2,1,0:T(8,128)(2,1)}, u32[]{:S(2)}) copy-start(bf16[8,256,256]{2,1,0:T(8,128)(2,1)} %param.19) | copy-start | bytes 3145732
  21.8 19.1 %copy-start.13 = (f32[2048]{0:T(1024)S(1)}, f32[2048]{0:T(1024)}, u32[]{:S(2)}) copy-start(f32[2048]{0:T(1024)} %param.21) | copy-start | bytes 24580
  21.8 19.2 %copy-start.12 = (f32[4,2048]{1,0:T(4,128)S(1)}, f32[4,2048]{1,0:T(4,128)}, u32[]{:S(2)}) copy-start(f32[4,2048]{1,0:T(4,128)} %param.18) | copy-start | bytes 98308
  23.4 21.0 %copy-start.15 = (f32[128,2]{0,1:T(2,128)S(1)}, f32[128,2]{0,1:T(2,128)}, u32[]{:S(2)}) copy-start(f32[128,2]{0,1:T(2,128)} %param.25) | copy-start | bytes 3076
  23.5 21.7 %copy-start.14 = (f32[128]{0:T(128)S(1)}, f32[128]{0:T(128)}, u32[]{:S(2)}) copy-start(f32[128]{0:T(128)} %param.22) | copy-start | bytes 1540
  23.5 63.4 %all-to-all-start = ((bf16[64,5,2048]{2,1,0:T(8,128)(2,1)}), bf16[64,5,2048]{2,1,0:T(8,128)(2,1)S(1)}, u32[]{:S(2)}, u32[]{:S(2)}) async-start(bf16[64,5,2048]{2,1,0:T(8,128)(2,1)} %broadcast_select_fusion.2), calls=%async_computation | async-start | bytes 4194304 | tf_op jit(solution)/shard_map/all_to_all | solution.py:194
  35.6 206.0 %reduce-scatter.2.cloned.1.call-start = ((), (), s32[]{:S(2)}) async-start(), calls=%async_computation.3 | async-start | bytes 6553600 | tf_op jit(solution)/shard_map/reduce_scatter | solution.py:198
  37.5 19.1 %collective-permute-start = (bf16[3,2048]{0,1:T(8,128)(2,1)}, bf16[3,2048]{0,1:T(8,128)(2,1)}, u32[]{:S(2)}, u32[]{:S(2)}) collective-permute-start(bf16[3,2048]{0,1:T(8,128)(2,1)} %copy.55), channel_id=1, source_target_pairs={{0,1},{1,2},{2,3},{3,4},{4,5},{5,6},{6,7},{7,8},{8,9},{9,10},{10,1... | collective-permute-start | bytes 36872 | tf_op jit(solution)/shard_map/ppermute | solution.py:34
  61.2 0.8 copy-start.5
  88.2 6.0 %copy-start.4 = (f32[128,8,256]{0,2,1:T(8,128)S(1)}, f32[128,8,256]{0,2,1:T(8,128)}, u32[]{:S(2)}) copy-start(f32[128,8,256]{0,2,1:T(8,128)} %copy.59) | copy-start | bytes 3145732
  88.2 30.6 %collective-permute-start.1 = (bf16[320,2048]{1,0:T(8,128)(2,1)}, bf16[320,2048]{1,0:T(8,128)(2,1)}, u32[]{:S(2)}, u32[]{:S(2)}) collective-permute-start(bf16[320,2048]{1,0:T(8,128)(2,1)} %reshape.838), channel_id=1, source_target_pairs={{0,1},{1,2},{2,3},{3,0},{4,5},{5,6},{6,7},{7,4},{8,9},{9,10},{10,1... | collective-permute-start | bytes 3932168 | tf_op jit(solution)/shard_map/ppermute | solution.py:21
  97.2 4.2 %copy-start.3 = (bf16[320,2048]{1,0:T(8,128)(2,1)S(1)}, bf16[320,2048]{1,0:T(8,128)(2,1)}, u32[]{:S(2)}) copy-start(bf16[320,2048]{1,0:T(8,128)(2,1)} %reshape.838) | copy-start | bytes 3932164
  101.4 30.9 %collective-permute-start.2 = (bf16[320,2048]{1,0:T(8,128)(2,1)S(1)}, bf16[320,2048]{1,0:T(8,128)(2,1)}, u32[]{:S(2)}, u32[]{:S(2)}) collective-permute-start(bf16[320,2048]{1,0:T(8,128)(2,1)S(1)} %copy-done.3), channel_id=1, source_target_pairs={{0,3},{1,0},{2,1},{3,2},{4,7},{5,4},{6,5},{7,6},{8,11},{9,8},{10,9... | collective-permute-start | bytes 3932168 | tf_op jit(solution)/shard_map/ppermute | solution.py:24
  118.8 29.7 %collective-permute-start.3 = (bf16[320,2048]{1,0:T(8,128)(2,1)}, bf16[320,2048]{1,0:T(8,128)(2,1)}, u32[]{:S(2)}, u32[]{:S(2)}) collective-permute-start(bf16[320,2048]{1,0:T(8,128)(2,1)} %collective-permute-done.1), channel_id=1, source_target_pairs={{0,1},{1,2},{2,3},{3,0},{4,5},{5,6},{6,7},{7,4},{8,9},{9,10},{10,1... | collective-permute-start | bytes 3932168 | tf_op jit(solution)/shard_map/ppermute | solution.py:21
  130.7 21.6 %copy-start.16 = (bf16[1,2048,896]{2,1,0:T(8,128)(2,1)S(1)}, bf16[1,2048,896]{2,1,0:T(8,128)(2,1)}, u32[]{:S(2)}) copy-start(bf16[1,2048,896]{2,1,0:T(8,128)(2,1)} %param.27) | copy-start | bytes 11010052
  150.0 2.4 copy-start.2
  177.1 0.9 copy-start.6
  177.1 1.0 copy-start.9
  177.1 1.0 copy-start.10
  241.6 13.6 %copy-start.7 = (bf16[128,2048]{1,0:T(8,128)(2,1)S(1)}, bf16[128,2048]{1,0:T(8,128)(2,1)}, u32[]{:S(2)}) copy-start(bf16[128,2048]{1,0:T(8,128)(2,1)} %param.16) | copy-start | bytes 1572868
  245.1 60.9 %all-to-all-start.1 = ((bf16[64,5,2048]{2,1,0:T(8,128)(2,1)}), bf16[64,5,2048]{2,1,0:T(8,128)(2,1)}, u32[]{:S(2)}, u32[]{:S(2)}) async-start(bf16[64,5,2048]{2,1,0:T(8,128)(2,1)} %reshape.839), calls=%async_computation.2 | async-start | bytes 4194304 | tf_op jit(solution)/shard_map/all_to_all | solution.py:204
  308.5 2.4 copy-start.8
  308.6 2.4 copy-start.11
  308.6 7.3 %copy-start.1 = (bf16[8,256,256]{2,1,0:T(8,128)(2,1)S(1)}, bf16[8,256,256]{2,1,0:T(8,128)(2,1)}, u32[]{:S(2)}) copy-start(bf16[8,256,256]{2,1,0:T(8,128)(2,1)} %param.19) | copy-start | bytes 3145732
Sparse Core Ops, SparseCore 0:
  177.2 58.1 reduce-scatter.1
